TPU v7x, 32 devices: a whole 2x2x4 slice. The times are simulated.
32 devices in a mesh: kv: 8 (over z, y), tp: 4 (over x, core).
Axes of the slice: x: 2, y: 2, z: 4, core: 2. Of those that a mesh axis runs over, the one named last changes fastest.
Arguments:
- hidden: bfloat16 [128, 4096], P(None, 'tp'), may hold values from -50 to 50
- input_gain: bfloat16 [4096], P('tp'), may hold values from 0.099609375 to 1.8984375
- x_weight: bfloat16 [4096, 8192], P('tp', 'kv'), may hold values from -0.09375 to 0.09375
- z_weight: bfloat16 [4096, 8192], P('tp', 'kv'), may hold values from -0.09375 to 0.09375
- bc_weight: bfloat16 [4096, 8192], P('tp', 'kv'), may hold values from -0.09375 to 0.09375
- dt_weight: bfloat16 [4096, 128], P('tp', 'kv'), may hold values from -0.09375 to 0.09375
- x_kernel: bfloat16 [4, 8192], P(None, 'kv'), may hold values from -3 to 3
- bc_kernel: bfloat16 [4, 8192], P(None, 'kv'), may hold values from -3 to 3
- dt_bias: float32 [128], P('kv'), may hold values from -3 to 0.5
- decay_log: float32 [128], P('kv'), may hold values from -3 to 1.5
- skip_scale: float32 [128], P('kv'), may hold values from 0.5 to 1.5
- output_gain: bfloat16 [8192], P('kv'), may hold values from 0.099609375 to 1.8984375
- output_weight: bfloat16 [8192, 4096], P('kv'), may hold values from -0.09375 to 0.09375
- saved_states: float32 [32, 5, 128, 64, 128], P('tp', None, 'kv'), may hold values from -1.8 to 1.8
- x_history: bfloat16 [32, 7, 8192], P('tp', None, 'kv'), may hold values from -6 to 6
- bc_history: bfloat16 [32, 7, 8192], P('tp', None, 'kv'), may hold values from -6 to 6
- accepted: int32 [32], P('tp'), may hold values from 0 to 4
Outputs:
- mixed: bfloat16 [128, 4096], P('tp', 'kv')
- new_states: float32 [32, 5, 128, 64, 128], P('tp', None, 'kv')
- x_window: bfloat16 [32, 7, 8192], P('tp', None, 'kv')
- bc_window: bfloat16 [32, 7, 8192], P('tp', None, 'kv')
All inputs are finite; a program needn't handle non-finite values.
Results may differ from a plain program's by a relative error of at most 0.02.
Values may be sent and summed in bfloat16 or wider, within the bound.
A program may use at most 192 MiB of HBM per device.

v0:
```python
import jax
import jax.numpy as jnp
import functools

from jax import lax
from jax.experimental import pallas as pl
from jax.experimental.pallas import tpu as pltpu
from jax.sharding import PartitionSpec as P

D = 4096
PROPS = 4
INNER = 8192


EPSILON = 1e-05


def partner_2(block, axis, stride):
    count = lax.axis_size(axis)
    route = []
    for low in range(count):
        high = low | 1 << stride
        if high != low and high < count:
            route += [(low, high), (high, low)]
    return lax.ppermute(block, axis, route)


def take_window(history, accepted, fresh_rows):
    history_len = history.shape[1] - fresh_rows.shape[1]
    indices = accepted[:, None] + jnp.arange(history_len, dtype=jnp.int32)[None, :]
    kept_rows = jnp.take_along_axis(history, indices[:, :, None], axis=1)
    return jnp.concatenate([kept_rows, fresh_rows], axis=1)


def conv_silu(window, kernel):
    length = window.shape[1] - kernel.shape[0] + 1
    running = window[:, 0:length].astype(jnp.float32) * kernel[0].astype(jnp.float32)
    for offset in range(1, kernel.shape[0]):
        running = running + window[:, offset : offset + length].astype(jnp.float32) * kernel[
            offset
        ].astype(jnp.float32)
    return jax.nn.silu(running)


def ssd_block(x_conv, step_size, decay_rate, b_terms, c_terms, first_state, skip_scale):
    cumulated = jnp.cumsum(-decay_rate * step_size, axis=1)
    length = x_conv.shape[1]
    indices = jnp.arange(length)
    causal = indices[:, None] >= indices[None, :]
    gaps = cumulated[:, :, None, :] - cumulated[:, None, :, :]
    weights = jnp.exp(jnp.where(causal[None, :, :, None], gaps, -jnp.inf))
    inputs = x_conv * step_size[..., None]
    outer_prod = jnp.einsum("srhp,srhn->srhpn", inputs, b_terms)
    states = jnp.exp(cumulated)[..., None, None] * first_state[:, None] + jnp.einsum(
        "strh,srhpn->sthpn", weights, outer_prod
    )
    output = jnp.einsum("sthn,sthpn->sthp", c_terms, states) + skip_scale[:, None] * x_conv
    return (output, states)


def local_general(
    hidden,
    input_gain,
    x_weight,
    z_weight,
    bc_weight,
    dt_weight,
    x_kernel,
    bc_kernel,
    dt_bias,
    decay_log,
    skip_scale,
    output_gain,
    output_weight,
    saved_states,
    x_history,
    bc_history,
    accepted,
):
    heads_here = dt_bias.shape[0]
    head_size = x_weight.shape[1] // heads_here
    state_size = saved_states.shape[4]
    seqs_here = accepted.shape[0]
    rows_here = hidden.shape[0] // lax.axis_size("tp")
    inner_here = x_weight.shape[1]
    bc_here = bc_weight.shape[1]
    widened = hidden.astype(jnp.float32)
    squares = lax.psum(jnp.sum(widened * widened, axis=1), "tp")
    normed = (
        widened * lax.rsqrt(squares[:, None] / D + EPSILON) * input_gain.astype(jnp.float32)
    ).astype(jnp.bfloat16)
    weights = jnp.concatenate([x_weight, z_weight, bc_weight, dt_weight], axis=1)
    product = jnp.dot(normed, weights, preferred_element_type=jnp.float32)
    projected = lax.psum_scatter(
        lax.optimization_barrier(product.astype(jnp.bfloat16))
        .astype(jnp.float32)
        .astype(jnp.bfloat16),
        "tp",
        scatter_dimension=0,
        tiled=True,
    )
    x_fresh = projected[:, :inner_here]
    z_fresh = projected[:, inner_here : 2 * inner_here]
    bc_fresh = projected[:, 2 * inner_here : 2 * inner_here + bc_here]
    dt_fresh = projected[:, 2 * inner_here + bc_here :]
    x_window = take_window(x_history, accepted, x_fresh.reshape(seqs_here, PROPS, inner_here))
    bc_window = take_window(bc_history, accepted, bc_fresh.reshape(seqs_here, PROPS, bc_here))
    x_conv = conv_silu(x_window, x_kernel).reshape(seqs_here, PROPS, heads_here, head_size)
    bc_conv = conv_silu(bc_window, bc_kernel)
    spread = max(4 // heads_here, 1)
    position = lax.axis_index("kv")
    for level in range(spread.bit_length() - 1):
        partner = partner_2(bc_conv, "kv", level)
        low_half = position // 2**level % 2 == 0
        bc_conv = jnp.where(
            low_half,
            jnp.concatenate([bc_conv, partner], axis=2),
            jnp.concatenate([partner, bc_conv], axis=2),
        )
    groups_here = bc_conv.shape[2] // (2 * state_size)
    paired = bc_conv.reshape(seqs_here, PROPS, groups_here, 2, state_size)
    per_group = heads_here // groups_here
    b_terms = jnp.repeat(paired[:, :, :, 0], per_group, axis=2)
    c_terms = jnp.repeat(paired[:, :, :, 1], per_group, axis=2)
    step_size = jax.nn.softplus(
        dt_fresh.astype(jnp.float32).reshape(seqs_here, PROPS, heads_here) + dt_bias
    )
    first_state = jnp.take_along_axis(saved_states, accepted[:, None, None, None, None], axis=1)[
        :, 0
    ]
    output, states = ssd_block(
        x_conv, step_size, jnp.exp(decay_log), b_terms, c_terms, first_state, skip_scale
    )
    new_states = jnp.concatenate([first_state[:, None], states], axis=1)
    gate_values = z_fresh.astype(jnp.float32).reshape(seqs_here, PROPS, heads_here, head_size)
    gated = (output * jax.nn.silu(gate_values)).reshape(rows_here, inner_here)
    square_sum = jnp.sum(gated * gated, axis=1)
    scaled = (gated * output_gain.astype(jnp.float32)).astype(jnp.bfloat16)
    partial_value = jnp.dot(scaled, output_weight, preferred_element_type=jnp.float32)
    total_squares = lax.psum(square_sum, "kv")
    summed = lax.psum_scatter(partial_value, "kv", scatter_dimension=1, tiled=True)
    mixed = (lax.rsqrt(total_squares / INNER + EPSILON)[:, None] * summed).astype(jnp.bfloat16)
    return (mixed, new_states, x_window, bc_window)


NN = (((1,), (0,)), ((), ()))
NT = (((1,), (1,)), ((), ()))
TN = (((0,), (0,)), ((), ()))


def dot(a, b, dims=NN, **kw):
    return lax.dot_general(a, b, dims, preferred_element_type=jnp.float32, **kw)


def silu(v):
    return v / (1.0 + jnp.exp(-v))


def softplus(v):
    return jnp.maximum(v, 0.0) + jnp.log(1.0 + jnp.exp(-jnp.abs(v)))


def mix_kernel(
    features, channels, n_out,
    acc_smem, bias_smem, decay_smem, skip_smem, proj_ref, xh_ref, bch_ref, xk_ref, bck_ref, gain_ref,
    saved_ref, w_ref,
    part_ref, xw_ref, bcw_ref, xdt_ref, b_ref, a_ref,
    s0_buf, w_buf, s0_sem, w_sem,
):
    seqs = acc_smem.shape[0]
    props = proj_ref.shape[0] // seqs
    rows = seqs * props
    inner = xh_ref.shape[2]
    bcw = bch_ref.shape[2]
    heads, size, state = s0_buf.shape[1:]
    groups = bcw // (2 * state)
    per = heads // groups
    span = per * size

    def s0_copy(s):
        return pltpu.make_async_copy(
            saved_ref.at[s, acc_smem[s]], s0_buf.at[s], s0_sem.at[s])

    for s in range(seqs):
        s0_copy(s).start()
    block = w_ref.shape[1] // n_out
    w_copies = [
        pltpu.make_async_copy(
            w_ref.at[:, pl.ds(i * block, block)], w_buf.at[i], w_sem.at[i])
        for i in range(n_out)
    ]
    for copy in w_copies:
        copy.start()

    ri = lax.broadcasted_iota(jnp.int32, (rows, rows), 0)
    ci = lax.broadcasted_iota(jnp.int32, (rows, rows), 1)
    to_steps = ((ri % seqs) * props + ri // seqs == ci).astype(jnp.float32).astype(jnp.bfloat16)
    back = ((ci % seqs) * props + ci // seqs == ri).astype(jnp.float32).astype(jnp.bfloat16)

    dt_at = 2 * inner + bcw
    last = proj_ref.shape[1]
    squares = proj_ref[:, last - 128 :].astype(jnp.float32)[:, 127:128]
    scale = lax.rsqrt(squares / features + EPSILON)

    def fresh(lo, hi):
        v = (proj_ref[:, lo:hi].astype(jnp.float32) * scale).astype(jnp.bfloat16)
        return dot(to_steps, v)

    def step(v, t):
        return v[t * seqs : (t + 1) * seqs]

    seq_at = lax.broadcasted_iota(jnp.int32, (seqs, inner), 0)
    acc = jnp.zeros((seqs, inner), jnp.int32)
    for s in range(seqs):
        acc = jnp.where(seq_at == s, acc_smem[s], acc)

    def window(hist_ref, rows_fresh, out_ref):
        kept = hist_ref.shape[0] - props
        hist = [hist_ref[m].astype(jnp.float32) for m in range(hist_ref.shape[0])]
        win = []
        for k in range(kept):
            v = hist[k]
            for j in range(1, props + 1):
                v = jnp.where(acc[:, :1] == j, hist[j + k], v)
            win.append(v)
        win += [step(rows_fresh, t) for t in range(props)]
        for m, v in enumerate(win):
            out_ref[m] = v.astype(jnp.bfloat16)
        return win

    def conv(win, kernel_ref):
        taps = [kernel_ref[j : j + 1].astype(jnp.float32) for j in range(kernel_ref.shape[0])]
        out = []
        for t in range(props):
            v = win[t] * taps[0]
            for j in range(1, len(taps)):
                v = v + win[t + j] * taps[j]
            out.append(silu(v))
        return out

    bc = conv(window(bch_ref, fresh(2 * inner, dt_at), bcw_ref), bck_ref)
    b_all = jnp.concatenate(
        [jnp.concatenate([v[:, 2 * g * state : (2 * g + 1) * state] for g in range(groups)], axis=1) for v in bc], axis=0)
    c_all = jnp.concatenate(
        [jnp.concatenate([v[:, (2 * g + 1) * state : (2 * g + 2) * state] for g in range(groups)], axis=1) for v in bc], axis=0)
    b_ref[...] = b_all.astype(jnp.bfloat16)
    c_low = c_all.astype(jnp.bfloat16)
    xc = conv(window(xh_ref, fresh(0, inner), xw_ref), xk_ref)

    dt_raw = fresh(dt_at, last)
    eh = lax.broadcasted_iota(jnp.int32, (128, inner), 0)
    ec = lax.broadcasted_iota(jnp.int32, (128, inner), 1)
    expand = (eh == ec // size).astype(jnp.float32)
    lane_at = lax.broadcasted_iota(jnp.int32, (8, 128), 1)
    row_at = lax.broadcasted_iota(jnp.int32, (8, 128), 0)
    par = jnp.zeros((8, 128), jnp.float32)
    for i, smem in enumerate((bias_smem, decay_smem, skip_smem)):
        for h in range(heads):
            par = jnp.where((row_at == i) & (lane_at == h), smem[h], par)
    wide = dot(par, expand, precision=lax.Precision.HIGHEST)
    dtw = dot(dt_raw.astype(jnp.bfloat16), expand.astype(jnp.bfloat16))
    lane = lax.broadcasted_iota(jnp.int32, (rows, 128), 1)
    raw = jnp.where(lane < heads, dt_raw, 0.0)
    a_ref[...] = jnp.exp(-jnp.exp(par[1:2]) * softplus(raw + par[0:1]))
    bias, rate, skip = wide[0:1], jnp.exp(wide[1:2]), wide[2:3]
    sizes = [softplus(step(dtw, t) + bias) for t in range(props)]
    xdt = [xc[t] * sizes[t] for t in range(props)]
    xdt_ref[...] = jnp.concatenate(xdt, axis=0).astype(jnp.bfloat16)

    row = lax.broadcasted_iota(jnp.int32, (rows, span), 0)
    carried = [jnp.zeros((rows, span), jnp.float32) for _ in range(groups)]
    for s in range(seqs):
        s0_copy(s).wait()
        for g in range(groups):
            s0 = s0_buf[s, g * per : (g + 1) * per].reshape(span, state).astype(jnp.bfloat16)
            got = dot(c_low[:, g * state : (g + 1) * state], s0, NT)
            carried[g] = jnp.where(row % seqs == s, got, carried[g])
    carried = jnp.concatenate(carried, axis=1)

    decays = [-rate * v for v in sizes]
    gated, sums = [], []
    zs = fresh(inner, 2 * inner)
    gain = gain_ref[...].astype(jnp.float32).reshape(1, inner)
    for t in range(props):
        total = decays[t]
        out = skip * xc[t]
        ct = step(c_all, t)
        for r in range(t, -1, -1):
            br = step(b_all, r)
            prod = ct * br
            pair = jnp.concatenate(
                [jnp.broadcast_to(
                    jnp.sum(prod[:, g * state : (g + 1) * state], axis=1, keepdims=True),
                    (seqs, span)) for g in range(groups)], axis=1)
            if r == t:
                out = out + pair * xdt[r]
            else:
                out = out + jnp.exp(total) * pair * xdt[r]
                total = total + decays[r]
        out = out + jnp.exp(total) * step(carried, t)
        v = out * silu(step(zs, t))
        gated.append((v * gain).astype(jnp.bfloat16))
        sums.append(jnp.broadcast_to(jnp.sum(v * v, axis=1, keepdims=True), (seqs, 128)))
    scaled = dot(back, jnp.concatenate(gated, axis=0)).astype(jnp.bfloat16)
    sums = jnp.concatenate(sums, axis=0)
    high = sums.astype(jnp.bfloat16)
    low = (sums - high.astype(jnp.float32)).astype(jnp.bfloat16)
    sums = dot(back, high) + dot(back, low)
    for i in range(n_out):
        w_copies[i].wait()
        part_ref[i, :, :block] = dot(scaled, w_buf[i]).astype(part_ref.dtype)
        part_ref[i, :, block:] = sums.astype(part_ref.dtype)


def state_kernel(acc_smem, a_smem, xdt_ref, b_ref, s0_ref, out_ref):
    s = pl.program_id(0)
    seqs = acc_smem.shape[0]
    rows = xdt_ref.shape[0]
    props = rows // seqs
    heads, size, state = s0_ref.shape[2:]
    groups = b_ref.shape[1] // state
    per = heads // groups
    row = lax.broadcasted_iota(jnp.int32, (rows, state), 0)
    first = s0_ref[0, 0]
    out_ref[0, 0] = first
    for g in range(groups):
        b = b_ref[:, g * state : (g + 1) * state].astype(jnp.float32)
        masked = jnp.concatenate(
            [jnp.where(row == t * seqs + s, b, 0.0) for t in range(props)], axis=1).astype(jnp.bfloat16)
        x = xdt_ref[:, g * per * size : (g + 1) * per * size]
        outer = dot(x, masked, TN)
        for h in range(per):
            head = g * per + h
            now = first[head]
            for t in range(props):
                now = a_smem[t * seqs + s, head] * now + outer[
                    h * size : (h + 1) * size, t * state : (t + 1) * state]
                out_ref[0, t + 1, head] = now


def exchange(axis, blocks_ref, slots, send_sems, recv_sems):
    count = blocks_ref.shape[0]
    me = lax.axis_index(axis)
    barrier = pltpu.get_barrier_semaphore()
    for d in range(1, count):
        pl.semaphore_signal(
            barrier, inc=1, device_id={axis: lax.rem(me + d, count)}, device_id_type=pl.DeviceIdType.MESH)
    pl.semaphore_wait(barrier, count - 1)
    copies = []
    for d in range(1, count):
        peer = lax.rem(me + d, count)
        copies.append(pltpu.make_async_remote_copy(
            src_ref=blocks_ref.at[peer],
            dst_ref=slots.at[d - 1],
            send_sem=send_sems.at[d - 1],
            recv_sem=recv_sems.at[d - 1],
            device_id={axis: peer},
            device_id_type=pl.DeviceIdType.MESH,
        ))
    for copy in copies:
        copy.start()
    total = blocks_ref[me].astype(jnp.float32)
    for d, copy in enumerate(copies):
        copy.wait_recv()
        total = total + slots[d].astype(jnp.float32)
    for copy in copies:
        copy.wait_send()
    return total


def entry_kernel(blocks_ref, out_ref, *scratch):
    out_ref[...] = exchange("tp", blocks_ref, *scratch)


def exit_kernel(channels, blocks_ref, out_ref, *scratch):
    total = exchange("kv", blocks_ref, *scratch)
    width = out_ref.shape[1]
    norm = lax.rsqrt(total[:, width : width + 1] / channels + EPSILON)
    out_ref[...] = (norm * total[:, :width]).astype(out_ref.dtype)


def exchange_call(body, name, number, blocks, out_shape):
    count = blocks.shape[0]
    return pl.pallas_call(
        body,
        out_shape=out_shape,
        in_specs=[pl.BlockSpec(memory_space=pltpu.VMEM)],
        out_specs=pl.BlockSpec(memory_space=pltpu.VMEM),
        scratch_shapes=[
            pltpu.VMEM((count - 1,) + blocks.shape[1:], blocks.dtype),
            pltpu.SemaphoreType.DMA((count - 1,)),
            pltpu.SemaphoreType.DMA((count - 1,)),
        ],
        compiler_params=pltpu.CompilerParams(collective_id=number, has_side_effects=True),
        name=name,
    )(blocks)


def local(
    hidden, input_gain, x_weight, z_weight, bc_weight, dt_weight, x_kernel, bc_kernel,
    dt_bias, decay_log, skip_scale, output_gain, output_weight, saved_states,
    x_history, bc_history, accepted,
):
    heads = dt_bias.shape[0]
    seqs, slots, _, size, state = saved_states.shape
    hist = x_history.shape[1]
    inner, bcw = x_weight.shape[1], bc_weight.shape[1]
    n_kv, n_tp = lax.axis_size("kv"), lax.axis_size("tp")
    rows = hidden.shape[0] // n_tp
    n_col = output_weight.shape[1]
    widened = hidden.astype(jnp.float32)
    squares = jnp.sum(widened * widened, axis=1, keepdims=True)
    entry = (widened * input_gain.astype(jnp.float32)).astype(jnp.bfloat16)
    weights = jnp.concatenate([x_weight, z_weight, bc_weight, dt_weight], axis=1)
    product = jnp.dot(entry, weights, preferred_element_type=jnp.float32).astype(jnp.bfloat16)
    fill = jnp.broadcast_to(squares.astype(jnp.bfloat16), (hidden.shape[0], 128 - heads))
    projected = exchange_call(
        entry_kernel, "entry_exchange", 0,
        jnp.concatenate([product, fill], axis=1).reshape(n_tp, rows, -1),
        jax.ShapeDtypeStruct((rows, product.shape[1] + 128 - heads), jnp.float32))

    vmem = pl.BlockSpec(memory_space=pltpu.VMEM)
    anym = pl.BlockSpec(memory_space=pl.ANY)
    smem = pl.BlockSpec(memory_space=pltpu.SMEM)
    block = n_col // n_kv
    part, xw, bcw_out, xdt, b, a = pl.pallas_call(
        functools.partial(mix_kernel, hidden.shape[1] * n_tp, inner * n_kv, n_kv),
        out_shape=(
            jax.ShapeDtypeStruct((n_kv, rows, block + 128), jnp.bfloat16),
            jax.ShapeDtypeStruct((hist, seqs, inner), jnp.bfloat16),
            jax.ShapeDtypeStruct((hist, seqs, bcw), jnp.bfloat16),
            jax.ShapeDtypeStruct((rows, inner), jnp.bfloat16),
            jax.ShapeDtypeStruct((rows, bcw // 2), jnp.bfloat16),
            jax.ShapeDtypeStruct((rows, 128), jnp.float32),
        ),
        in_specs=[smem] * 4 + [vmem] * 6 + [anym] * 2,
        out_specs=[vmem] * 6,
        scratch_shapes=[
            pltpu.VMEM((seqs, heads, size, state), jnp.float32),
            pltpu.VMEM((n_kv, inner, block), jnp.bfloat16),
            pltpu.SemaphoreType.DMA((seqs,)),
            pltpu.SemaphoreType.DMA((n_kv,)),
        ],
        compiler_params=pltpu.CompilerParams(vmem_limit_bytes=60 << 20),
        cost_estimate=pl.CostEstimate(
            flops=2 * rows * inner * n_col, bytes_accessed=14 << 20, transcendentals=0),
        name="mix",
    )(
        accepted, dt_bias, decay_log, skip_scale, projected,
        x_history.transpose(1, 0, 2), bc_history.transpose(1, 0, 2),
        x_kernel, bc_kernel, output_gain, saved_states, output_weight,
    )
    mixed = exchange_call(
        functools.partial(exit_kernel, inner * n_kv), "exit_exchange", 1, part,
        jax.ShapeDtypeStruct((rows, block), jnp.bfloat16))

    new_states = pl.pallas_call(
        state_kernel,
        out_shape=jax.ShapeDtypeStruct(saved_states.shape, jnp.float32),
        grid_spec=pltpu.PrefetchScalarGridSpec(
            num_scalar_prefetch=1,
            grid=(seqs,),
            in_specs=[
                smem,
                pl.BlockSpec((rows, inner), lambda s, acc: (0, 0)),
                pl.BlockSpec((rows, bcw // 2), lambda s, acc: (0, 0)),
                pl.BlockSpec((1, 1, heads, size, state), lambda s, acc: (s, acc[s], 0, 0, 0)),
            ],
            out_specs=pl.BlockSpec((1, slots, heads, size, state), lambda s, acc: (s, 0, 0, 0, 0)),
        ),
        compiler_params=pltpu.CompilerParams(vmem_limit_bytes=60 << 20),
        cost_estimate=pl.CostEstimate(
            flops=2 * saved_states.size, bytes_accessed=6 * saved_states.size, transcendentals=0),
        name="states",
    )(accepted, a, xdt, b, saved_states)

    return (mixed, new_states, xw.transpose(1, 0, 2), bcw_out.transpose(1, 0, 2))


def fits(mesh):
    inner = INNER // mesh.shape["kv"]
    return inner % 1024 == 0 and mesh.shape["kv"] > 1


def solution(mesh):
    in_specs = (
        P(None, "tp"),
        P("tp"),
        P("tp", "kv"),
        P("tp", "kv"),
        P("tp", "kv"),
        P("tp", "kv"),
        P(None, "kv"),
        P(None, "kv"),
        P("kv"),
        P("kv"),
        P("kv"),
        P("kv"),
        P("kv", None),
        P("tp", None, "kv", None, None),
        P("tp", None, "kv"),
        P("tp", None, "kv"),
        P("tp"),
    )
    out_specs = (
        P("tp", "kv"),
        P("tp", None, "kv", None, None),
        P("tp", None, "kv"),
        P("tp", None, "kv"),
    )
    body = local if fits(mesh) else local_general
    return jax.shard_map(body, mesh=mesh, in_specs=in_specs, out_specs=out_specs, check_vma=False)
```

profile of v0, /device:TPU:0, one launch (start us, length us, event | category | flops | bytes accessed | tf_op | source)
XLA Modules:
  0.0 58.8 jit_solution(17094234568084997740)
XLA Ops:
  0.6 1.1 %fusion.12 = bf16[128]{0:T(256)(128)(2,1)S(1)} fusion(bf16[128,1024]{1,0:T(8,128)(2,1)} %param.17), kind=kLoop, calls=%fused_computation.13 | loop fusion | flops 393088 | bytes 262400 | tf_op jit(solution)/shard_map/reduce_sum | solution.py:412
  1.7 0.7 %convert_element_type.21 = f32[1024]{0:T(1024)S(1)} convert(bf16[1024]{0:T(1024)(128)(2,1)} %param.18) | non-fusion elementwise | flops 1024 | bytes 6144 | tf_op jit(solution)/shard_map/convert_element_type | solution.py:413
  2.4 0.9 %copy.21 = bf16[1024,16]{1,0:T(8,128)(2,1)S(1)} copy(bf16[1024,16]{0,1:T(8,128)(2,1)} %param.22) | data formatting | bytes 65536 | tf_op args[5]
  3.3 5.6 %fusion.8 = bf16[128,3088]{0,1:T(8,128)(2,1)S(1)} fusion(bf16[1024,16]{1,0:T(8,128)(2,1)S(1)} %copy.21, bf16[1024,1024]{1,0:T(8,128)(2,1)} %param.21, bf16[1024,1024]{1,0:T(8,128)(2,1)} %param.20, bf16[1024,1024]{1,0:T(8,128)(2,1)} %param.19, bf16[128,1024]{1,0:T(8,128)(2,1)} %param.17, f32[1024]{0:T(1024)S(1)} %convert_element_type.21), kind=kOutput, calls=%fused_computation.8 | convolution fusion | flops 835586048 | bytes 7380992 | tf_op jit(solution)/shard_map/dot_general | solution.py:415
  8.9 0.1 pad_maximum_fusion
  9.0 1.5 %copy.22 = bf16[128,3200]{1,0:T(8,128)(2,1)} copy(bf16[128,3200]{0,1:T(8,128)(2,1)S(1)} %pad_maximum_fusion) | data formatting | bytes 1638400 | tf_op jit(solution)/shard_map/concatenate | solution.py:419
  10.5 14.2 %entry_exchange.1.proj_ref = f32[32,3200]{1,0:T(8,128)} custom-call(bf16[4,32,3200]{2,1,0:T(8,128)(2,1)} %bitcast.5), custom_call_target="tpu_custom_call" | custom-call | tf_op jit(solution)/shard_map/entry_exchange/pallas_call | solution.py:384
  24.7 9.2 %mix.1 = (bf16[8,32,640]{2,1,0:T(8,128)(2,1)}, bf16[7,8,1024]{2,1,0:T(8,128)(2,1)}, bf16[7,8,1024]{2,1,0:T(8,128)(2,1)}, bf16[32,1024]{1,0:T(8,128)(2,1)}, bf16[32,512]{1,0:T(8,128)(2,1)}, /*index=5*/f32[32,128]{1,0:T(8,128)}) custom-call(s32[8]{0:T(128)} %acc_smem.3, f32[16]{0:T(128)} %bias_smem.1, f32[16]{0:T(128)} %decay_smem.1, f32[16]{0:T(128)} %skip_smem.1, ...), custom_call_target="tpu_custom_call" | custom-call | flops 268435456 | bytes 14680064 | tf_op jit(solution)/shard_map/mix/pallas_call | solution.py:426
  33.9 12.8 %exit_exchange.1 = bf16[32,512]{1,0:T(8,128)(2,1)} custom-call(bf16[8,32,640]{2,1,0:T(8,128)(2,1)} %get-tuple-element.10.blocks_ref), custom_call_target="tpu_custom_call" | custom-call | tf_op jit(solution)/shard_map/exit_exchange/pallas_call | solution.py:384
  46.6 0.0 copy-start
  46.7 11.5 %states.1 = f32[8,5,16,64,128]{4,3,2,1,0:T(8,128)} custom-call(s32[8]{0:T(128)} %acc_smem.3, f32[32,128]{1,0:T(8,128)} %get-tuple-element.11.a_smem, bf16[32,1024]{1,0:T(8,128)(2,1)} %get-tuple-element.12.xdt_ref, bf16[32,512]{1,0:T(8,128)(2,1)} %get-tuple-element.13.b_ref, f32[8,5,16,64,128]{4,3,2,1,0:T(8,128)} %s0_ref.1), custom_call_target="tpu_custom_call" | custom-call | flops 10485760 | bytes 31457280 | tf_op jit(solution)/shard_map/states/pallas_call | solution.py:457
  58.2 0.0 copy-done
  58.2 0.6 %copy.24 = bf16[32,512]{1,0:T(8,128)(2,1)} copy(bf16[32,512]{1,0:T(8,128)(2,1)S(1)} %copy-done) | data formatting | bytes 65536
  (1 shorter events, 0.0 us)
Async XLA Ops:
  46.6 11.5 %copy-start = (bf16[32,512]{1,0:T(8,128)(2,1)S(1)}, bf16[32,512]{1,0:T(8,128)(2,1)}, u32[]{:S(2)}) copy-start(bf16[32,512]{1,0:T(8,128)(2,1)} %exit_exchange.1) | copy-start | bytes 98308
where the time goes:
time: 59.8 us; the launch traced here: 58.8 us
  Pallas kernels  47.7 us (80%)
  matrix products  5.59 us (9%)
  local copies, waits for them, and re-layouts  3.01 us (5%)
  other arithmetic  1.83 us (3%)
  between operations  0.68 us (1%)
    pallas_call x2, Pallas kernels, exchange_call(): pl.pallas_call(body, out_shape=out_shape, in_specs=[pl.BlockSpec(memory_s...  27 us
    pallas_call x1, Pallas kernels, local(): pl.pallas_call(state_kernel, out_shape=jax.ShapeDtypeStruct(saved_states....  11.5 us
    pallas_call x1, Pallas kernels, local(): pl.pallas_call(functools.partial(mix_kernel, hidden.shape[1] * n_tp, inne...  9.17 us
    dot_general x1, matrix products, local(): jnp.dot(entry, weights, preferred_element_type=jnp.float32)  5.59 us
    unnamed x4, local copies, waits for them, and re-layouts  1.54 us
    concatenate x1, local copies, waits for them, and re-layouts, local(): jnp.concatenate([product, fill], axis=1).reshape(n_tp, rows, -1)  1.46 us

commit v1 on v0

v1 whole, which is shorter than its diff:
```python
import jax
import jax.numpy as jnp
import functools

from jax import lax
from jax.experimental import pallas as pl
from jax.experimental.pallas import tpu as pltpu
from jax.sharding import PartitionSpec as P

D = 4096
PROPS = 4
INNER = 8192


EPSILON = 1e-05


def partner_2(block, axis, stride):
    count = lax.axis_size(axis)
    route = []
    for low in range(count):
        high = low | 1 << stride
        if high != low and high < count:
            route += [(low, high), (high, low)]
    return lax.ppermute(block, axis, route)


def take_window(history, accepted, fresh_rows):
    history_len = history.shape[1] - fresh_rows.shape[1]
    indices = accepted[:, None] + jnp.arange(history_len, dtype=jnp.int32)[None, :]
    kept_rows = jnp.take_along_axis(history, indices[:, :, None], axis=1)
    return jnp.concatenate([kept_rows, fresh_rows], axis=1)


def conv_silu(window, kernel):
    length = window.shape[1] - kernel.shape[0] + 1
    running = window[:, 0:length].astype(jnp.float32) * kernel[0].astype(jnp.float32)
    for offset in range(1, kernel.shape[0]):
        running = running + window[:, offset : offset + length].astype(jnp.float32) * kernel[
            offset
        ].astype(jnp.float32)
    return jax.nn.silu(running)


def ssd_block(x_conv, step_size, decay_rate, b_terms, c_terms, first_state, skip_scale):
    cumulated = jnp.cumsum(-decay_rate * step_size, axis=1)
    length = x_conv.shape[1]
    indices = jnp.arange(length)
    causal = indices[:, None] >= indices[None, :]
    gaps = cumulated[:, :, None, :] - cumulated[:, None, :, :]
    weights = jnp.exp(jnp.where(causal[None, :, :, None], gaps, -jnp.inf))
    inputs = x_conv * step_size[..., None]
    outer_prod = jnp.einsum("srhp,srhn->srhpn", inputs, b_terms)
    states = jnp.exp(cumulated)[..., None, None] * first_state[:, None] + jnp.einsum(
        "strh,srhpn->sthpn", weights, outer_prod
    )
    output = jnp.einsum("sthn,sthpn->sthp", c_terms, states) + skip_scale[:, None] * x_conv
    return (output, states)


def local_general(
    hidden,
    input_gain,
    x_weight,
    z_weight,
    bc_weight,
    dt_weight,
    x_kernel,
    bc_kernel,
    dt_bias,
    decay_log,
    skip_scale,
    output_gain,
    output_weight,
    saved_states,
    x_history,
    bc_history,
    accepted,
):
    heads_here = dt_bias.shape[0]
    head_size = x_weight.shape[1] // heads_here
    state_size = saved_states.shape[4]
    seqs_here = accepted.shape[0]
    rows_here = hidden.shape[0] // lax.axis_size("tp")
    inner_here = x_weight.shape[1]
    bc_here = bc_weight.shape[1]
    widened = hidden.astype(jnp.float32)
    squares = lax.psum(jnp.sum(widened * widened, axis=1), "tp")
    normed = (
        widened * lax.rsqrt(squares[:, None] / D + EPSILON) * input_gain.astype(jnp.float32)
    ).astype(jnp.bfloat16)
    weights = jnp.concatenate([x_weight, z_weight, bc_weight, dt_weight], axis=1)
    product = jnp.dot(normed, weights, preferred_element_type=jnp.float32)
    projected = lax.psum_scatter(
        lax.optimization_barrier(product.astype(jnp.bfloat16))
        .astype(jnp.float32)
        .astype(jnp.bfloat16),
        "tp",
        scatter_dimension=0,
        tiled=True,
    )
    x_fresh = projected[:, :inner_here]
    z_fresh = projected[:, inner_here : 2 * inner_here]
    bc_fresh = projected[:, 2 * inner_here : 2 * inner_here + bc_here]
    dt_fresh = projected[:, 2 * inner_here + bc_here :]
    x_window = take_window(x_history, accepted, x_fresh.reshape(seqs_here, PROPS, inner_here))
    bc_window = take_window(bc_history, accepted, bc_fresh.reshape(seqs_here, PROPS, bc_here))
    x_conv = conv_silu(x_window, x_kernel).reshape(seqs_here, PROPS, heads_here, head_size)
    bc_conv = conv_silu(bc_window, bc_kernel)
    spread = max(4 // heads_here, 1)
    position = lax.axis_index("kv")
    for level in range(spread.bit_length() - 1):
        partner = partner_2(bc_conv, "kv", level)
        low_half = position // 2**level % 2 == 0
        bc_conv = jnp.where(
            low_half,
            jnp.concatenate([bc_conv, partner], axis=2),
            jnp.concatenate([partner, bc_conv], axis=2),
        )
    groups_here = bc_conv.shape[2] // (2 * state_size)
    paired = bc_conv.reshape(seqs_here, PROPS, groups_here, 2, state_size)
    per_group = heads_here // groups_here
    b_terms = jnp.repeat(paired[:, :, :, 0], per_group, axis=2)
    c_terms = jnp.repeat(paired[:, :, :, 1], per_group, axis=2)
    step_size = jax.nn.softplus(
        dt_fresh.astype(jnp.float32).reshape(seqs_here, PROPS, heads_here) + dt_bias
    )
    first_state = jnp.take_along_axis(saved_states, accepted[:, None, None, None, None], axis=1)[
        :, 0
    ]
    output, states = ssd_block(
        x_conv, step_size, jnp.exp(decay_log), b_terms, c_terms, first_state, skip_scale
    )
    new_states = jnp.concatenate([first_state[:, None], states], axis=1)
    gate_values = z_fresh.astype(jnp.float32).reshape(seqs_here, PROPS, heads_here, head_size)
    gated = (output * jax.nn.silu(gate_values)).reshape(rows_here, inner_here)
    square_sum = jnp.sum(gated * gated, axis=1)
    scaled = (gated * output_gain.astype(jnp.float32)).astype(jnp.bfloat16)
    partial_value = jnp.dot(scaled, output_weight, preferred_element_type=jnp.float32)
    total_squares = lax.psum(square_sum, "kv")
    summed = lax.psum_scatter(partial_value, "kv", scatter_dimension=1, tiled=True)
    mixed = (lax.rsqrt(total_squares / INNER + EPSILON)[:, None] * summed).astype(jnp.bfloat16)
    return (mixed, new_states, x_window, bc_window)


NN = (((1,), (0,)), ((), ()))
NT = (((1,), (1,)), ((), ()))
CHUNK = 512
LAG = 3


def dot(a, b, dims=NN, **kw):
    return lax.dot_general(a, b, dims, preferred_element_type=jnp.float32, **kw)


def silu(v):
    return v / (1.0 + jnp.exp(-v))


def softplus(v):
    return jnp.maximum(v, 0.0) + jnp.log(1.0 + jnp.exp(-jnp.abs(v)))


def flip(index, mask):
    out = index
    bit = 1
    while bit <= mask:
        if mask & bit:
            out = out + bit - 2 * bit * lax.rem(index // bit, 2)
        bit *= 2
    return out


def remote(src, dst, send_sem, recv_sem, device):
    return pltpu.make_async_remote_copy(
        src_ref=src, dst_ref=dst, send_sem=send_sem, recv_sem=recv_sem,
        device_id=device, device_id_type=pl.DeviceIdType.MESH)


def main_kernel(
    features, channels, n_kv,
    acc_smem, bias_smem, decay_smem, skip_smem,
    hid_hbm, gin_ref, xw_hbm, zw_hbm, bcw_hbm, dtw_hbm, xh_ref, bch_ref, xk_ref, bck_ref, gain_ref,
    saved_hbm, w_hbm,
    mixed_ref, s0_ref, xdt_ref, b_ref, a_ref, xwin_ref, bcwin_ref,
    hid, entry32, dtw, wbuf, prod_dt, prod, peer_dt, peer, half_dt, half, own_dt, own, far_dt, far,
    w_buf, part, slots, norm_out, norm_in, fin,
    hid_sem, w_sem, saved_sem, ow_sem, c_send, c_recv, x_send, x_recv, o_send, o_recv, n_send, n_recv,
    *saved,
):
    seqs = acc_smem.shape[0]
    rows = mixed_ref.shape[0]
    props = rows // seqs
    tokens = hid.shape[0]
    inner = xwin_ref.shape[2]
    _, heads, size, state = saved[0].shape
    groups = bcwin_ref.shape[2] // (2 * state)
    per = heads // groups
    span = per * size
    n_chunk = inner // CHUNK
    in_chunk = CHUNK // span
    block = mixed_ref.shape[1]

    kv, tp = lax.axis_index("kv"), lax.axis_index("tp")
    side, core = tp // 2, lax.rem(tp, 2)
    core_peer, x_peer = flip(tp, 1), flip(tp, 2)
    exits = [flip(kv, d) for d in range(n_kv - 1, 0, -1)]

    barrier = pltpu.get_barrier_semaphore()
    for device in [{"tp": core_peer}, {"tp": x_peer}] + [{"kv": p} for p in exits]:
        pl.semaphore_signal(barrier, inc=1, device_id=device, device_id_type=pl.DeviceIdType.MESH)

    hid_copy = pltpu.make_async_copy(hid_hbm, hid, hid_sem.at[0])
    hid_copy.start()
    dtw_copy = pltpu.make_async_copy(dtw_hbm, dtw.at[pl.ds(0, heads)], hid_sem.at[1])
    dtw_copy.start()
    w_copies = [
        pltpu.make_async_copy(src.at[:, pl.ds(j * CHUNK, CHUNK)], wbuf.at[i], w_sem.at[i])
        for i, (src, j) in enumerate(
            [(src, j) for src in (bcw_hbm, xw_hbm, zw_hbm) for j in range(n_chunk)])
    ]
    for copy in w_copies:
        copy.start()
    n_big = len(w_copies)

    dtw[heads:] = jnp.zeros((dtw.shape[0] - heads, dtw.shape[1]), dtw.dtype)
    hid_copy.wait()
    lanes = entry32.shape[2]
    for i in range(entry32.shape[0]):
        entry32[i] = hid[:, i * lanes : (i + 1) * lanes].astype(jnp.float32)
    gin = gin_ref[...].astype(jnp.float32).reshape(1, -1)
    entry, squares = [], []
    for p in range(tokens // rows):
        for t in range(props):
            v = jnp.concatenate(
                [entry32[i, pl.ds(p * rows + t, seqs, stride=props), :] for i in range(entry32.shape[0])],
                axis=1)
            squares.append(jnp.sum(v * v, axis=1, keepdims=True))
            entry.append(v * gin)
    entry = jnp.concatenate(entry, axis=0).astype(jnp.bfloat16)
    squares = jnp.concatenate(squares, axis=0)
    high = squares.astype(jnp.bfloat16).astype(jnp.float32)

    saved_copies = [
        pltpu.make_async_copy(saved_hbm.at[s], saved[s], saved_sem.at[s]) for s in range(seqs)]
    ow_copies = [
        pltpu.make_async_copy(
            w_hbm.at[:, pl.ds(pl.multiple_of(p * block, block), block)], w_buf.at[i], ow_sem.at[i])
        for i, p in enumerate(exits + [kv])]

    def put(ref, value):
        for p in range(tokens // rows):
            ref[(p % 2) * 2 + p // 2] = value[p * rows : (p + 1) * rows].astype(jnp.bfloat16)

    def core_copy(k):
        src, dst = (prod_dt, peer_dt) if k < 0 else (prod.at[k], peer.at[k])
        return remote(
            src.at[pl.ds(2 - 2 * core, 2)], dst, c_send.at[k + 1], c_recv.at[k + 1], {"tp": core_peer})

    def x_copy(k):
        src, dst = (half_dt, far_dt) if k < 0 else (half.at[k], far.at[k])
        return remote(src, dst, x_send.at[k + 1], x_recv.at[k + 1], {"tp": x_peer})

    def forward(k):
        core_copy(k).wait_recv()
        mine, theirs, send, keep = (prod_dt, peer_dt, half_dt, own_dt) if k < 0 else (
            prod.at[k], peer.at[k], half.at[k], own.at[k])
        away = mine[2 * core + 1 - side].astype(jnp.float32) + theirs[1 - side].astype(jnp.float32)
        send[...] = away.astype(jnp.bfloat16)
        x_copy(k).start()
        keep[...] = mine[2 * core + side].astype(jnp.float32) + theirs[side].astype(jnp.float32)

    dtw_copy.wait()
    lane = lax.broadcasted_iota(jnp.int32, (tokens, 128), 1)
    first = dot(entry, dtw[...], NT)
    first = jnp.where(lane == 126, high, jnp.where(lane == 127, squares - high, first))
    put(prod_dt, first)
    pl.semaphore_wait(barrier, 2 + len(exits))
    core_copy(-1).start()
    for k in range(n_big):
        w_copies[k].wait()
        put(prod.at[k], dot(entry, wbuf[k]))
        core_copy(k).start()
        if k >= LAG - 1:
            forward(k - LAG)
        if k == n_big - 1:
            for copy in saved_copies + ow_copies:
                copy.start()
    for k in range(n_big - LAG, n_big):
        forward(k)

    seq_at = lax.broadcasted_iota(jnp.int32, (seqs, CHUNK), 0)
    acc = jnp.zeros((seqs, CHUNK), jnp.int32)
    for s in range(seqs):
        acc = jnp.where(seq_at == s, acc_smem[s], acc)
    picks = [acc == j for j in range(props + 1)]
    eh = lax.broadcasted_iota(jnp.int32, (128, inner), 0)
    ec = lax.broadcasted_iota(jnp.int32, (128, inner), 1)
    expand = (eh == ec // size).astype(jnp.float32)
    lane_at = lax.broadcasted_iota(jnp.int32, (8, 128), 1)
    row_at = lax.broadcasted_iota(jnp.int32, (8, 128), 0)
    par = jnp.zeros((8, 128), jnp.float32)
    for i, smem in enumerate((bias_smem, decay_smem, skip_smem)):
        for h in range(heads):
            par = jnp.where((row_at == i) & (lane_at == h), smem[h], par)
    wide = dot(par, expand, precision=lax.Precision.HIGHEST)
    bias, rate, skip = wide[0:1], jnp.exp(wide[1:2]), wide[2:3]
    row = lax.broadcasted_iota(jnp.int32, (rows, state), 0)

    def total(k):
        x_copy(k).wait_recv()
        if k < 0:
            return own_dt[...] + far_dt[...].astype(jnp.float32)
        return own[k] + far[k].astype(jnp.float32)

    head_part = total(-1)
    sums = head_part[:, 126:127] + head_part[:, 127:128]
    scale = lax.rsqrt(sums / features + EPSILON)

    def fresh(k):
        v = (total(k) * scale).astype(jnp.bfloat16).astype(jnp.float32)
        return [v[t * seqs : (t + 1) * seqs] for t in range(props)]

    def conv(hist_ref, tap_ref, out_ref, rows_fresh, lo):
        kept = hist_ref.shape[0] - props
        hist = [hist_ref[m, :, lo : lo + CHUNK].astype(jnp.float32) for m in range(hist_ref.shape[0])]
        win = []
        for k in range(kept):
            v = hist[k]
            for j in range(1, props + 1):
                v = jnp.where(picks[j], hist[j + k], v)
            win.append(v)
        win += rows_fresh
        for m, v in enumerate(win):
            out_ref[m, :, lo : lo + CHUNK] = v.astype(jnp.bfloat16)
        taps = [tap_ref[j : j + 1, lo : lo + CHUNK].astype(jnp.float32) for j in range(tap_ref.shape[0])]
        out = []
        for t in range(props):
            v = win[t] * taps[0]
            for j in range(1, len(taps)):
                v = v + win[t + j] * taps[j]
            out.append(silu(v))
        return out

    dt_raw = (head_part * scale).astype(jnp.bfloat16)
    dtw_wide = dot(dt_raw, expand.astype(jnp.bfloat16))
    head_lane = lax.broadcasted_iota(jnp.int32, (rows, 128), 1)
    raw = jnp.where(head_lane < heads, dt_raw.astype(jnp.float32), 0.0)
    a_ref[...] = jnp.exp(-jnp.exp(par[1:2]) * softplus(raw + par[0:1]))

    b_terms, c_low, pairs = [], [], []
    for j in range(n_chunk):
        bc = conv(bch_ref, bck_ref, bcwin_ref, fresh(j), j * CHUNK)
        for i in range(CHUNK // (2 * state)):
            b = [v[:, 2 * i * state : (2 * i + 1) * state] for v in bc]
            c = [v[:, (2 * i + 1) * state : (2 * i + 2) * state] for v in bc]
            g = len(c_low)
            b_ref[:, g * state : (g + 1) * state] = jnp.concatenate(b, axis=0).astype(jnp.bfloat16)
            c_low.append(jnp.concatenate(c, axis=0).astype(jnp.bfloat16))
            pairs.append({
                (t, r): jnp.broadcast_to(jnp.sum(c[t] * b[r], axis=1, keepdims=True), (seqs, span))
                for t in range(props) for r in range(t + 1)})

    carried = [jnp.zeros((rows, span), jnp.float32) for _ in range(groups)]
    for s in range(seqs):
        saved_copies[s].wait()
        s0 = saved[s][acc_smem[s]]
        s0_ref[s] = s0
        low = s0.reshape(heads * size, state).astype(jnp.bfloat16)
        for g in range(groups):
            masked = jnp.where(row % seqs == s, c_low[g].astype(jnp.float32), 0.0).astype(jnp.bfloat16)
            carried[g] = carried[g] + dot(masked, low[g * span : (g + 1) * span], NT)

    outs, gated_parts = [], []
    for j in range(n_chunk):
        lo = j * CHUNK
        sl = slice(lo, lo + CHUNK)
        xc = conv(xh_ref, xk_ref, xwin_ref, fresh(n_chunk + j), lo)
        sizes = [
            softplus(dtw_wide[t * seqs : (t + 1) * seqs, sl] + bias[:, sl]) for t in range(props)]
        xdt = [xc[t] * sizes[t] for t in range(props)]
        xdt_ref[:, sl] = jnp.concatenate(xdt, axis=0).astype(jnp.bfloat16)
        decays = [-rate[:, sl] * v for v in sizes]
        out_t = []
        for t in range(props):
            gap = decays[t]
            out = skip[:, sl] * xc[t]
            for r in range(t, -1, -1):
                pair = jnp.concatenate(
                    [pairs[j * in_chunk + i][(t, r)] for i in range(in_chunk)], axis=1)
                if r == t:
                    out = out + pair * xdt[r]
                else:
                    out = out + jnp.exp(gap) * pair * xdt[r]
                    gap = gap + decays[r]
            held = jnp.concatenate(
                [carried[j * in_chunk + i][t * seqs : (t + 1) * seqs] for i in range(in_chunk)], axis=1)
            out_t.append(out + jnp.exp(gap) * held)
        outs.append(out_t)
    square_sums = [jnp.zeros((seqs, 1), jnp.float32) for _ in range(props)]
    gain = gain_ref[...].astype(jnp.float32).reshape(1, inner)
    for j in range(n_chunk):
        sl = slice(j * CHUNK, (j + 1) * CHUNK)
        zs = fresh(2 * n_chunk + j)
        scaled_t = []
        for t in range(props):
            v = outs[j][t] * silu(zs[t])
            square_sums[t] = square_sums[t] + jnp.sum(v * v, axis=1, keepdims=True)
            scaled_t.append((v * gain[:, sl]).astype(jnp.bfloat16))
        gated_parts.append(jnp.concatenate(scaled_t, axis=0))
    scaled = jnp.concatenate(gated_parts, axis=1)

    diagonal = lax.broadcasted_iota(jnp.int32, (rows, 128), 0) == lax.broadcasted_iota(
        jnp.int32, (rows, 128), 1)
    norm_row = jnp.sum(
        jnp.where(diagonal, jnp.concatenate(square_sums, axis=0), 0.0), axis=0, keepdims=True)
    norm_out[...] = norm_row
    n_copies = [
        remote(norm_out, norm_in.at[i], n_send.at[i], n_recv.at[i], {"kv": p})
        for i, p in enumerate(exits)]
    for copy in n_copies:
        copy.start()
    o_copies = [
        remote(part.at[i], slots.at[i], o_send.at[i], o_recv.at[i], {"kv": p})
        for i, p in enumerate(exits)]
    for i in range(n_kv):
        ow_copies[i].wait()
        value = dot(scaled, w_buf[i])
        if i < n_kv - 1:
            part[i] = value.astype(jnp.bfloat16)
            o_copies[i].start()
    for copy in n_copies:
        copy.wait_recv()
    for i in range(n_kv - 1):
        norm_row = norm_row + norm_in[i]
    norm = lax.rsqrt(
        jnp.sum(jnp.where(diagonal, norm_row, 0.0), axis=1, keepdims=True) / channels + EPSILON)
    for i in range(n_kv - 2, -1, -1):
        o_copies[i].wait_recv()
        value = value + slots[i].astype(jnp.float32)
    value = value * norm
    for i in range(fin.shape[0]):
        for t in range(props):
            fin[i, pl.ds(t, seqs, stride=props), :] = value[
                t * seqs : (t + 1) * seqs, i * lanes : (i + 1) * lanes]
        mixed_ref[:, i * lanes : (i + 1) * lanes] = fin[i].astype(mixed_ref.dtype)
    for k in range(-1, n_big):
        core_copy(k).wait_send()
        x_copy(k).wait_send()
    for copy in n_copies + o_copies:
        copy.wait_send()


def write_kernel(
    mixed_ref, s0_ref, xdt_ref, b_ref, a_ref, xwin_ref, bcwin_ref,
    mixed_out, states_out, xwin_out, bcwin_out,
    a_smem, new, a_sem, small_sem, first_sem, new_sem,
):
    seqs, heads, size, state = s0_ref.shape
    rows = b_ref.shape[0]
    props = rows // seqs
    groups = b_ref.shape[1] // state
    per = heads // groups
    span = per * size
    a_copy = pltpu.make_async_copy(a_ref, a_smem, a_sem)
    a_copy.start()
    copies = [
        pltpu.make_async_copy(s0_ref.at[s], states_out.at[s, 0], first_sem.at[s]) for s in range(seqs)]
    copies += [
        pltpu.make_async_copy(src, dst, small_sem.at[i])
        for i, (src, dst) in enumerate(
            [(mixed_ref, mixed_out), (xwin_ref, xwin_out), (bcwin_ref, bcwin_out)])]
    for copy in copies:
        copy.start()
    row = lax.broadcasted_iota(jnp.int32, (rows, state), 0)
    a_copy.wait()
    turned = [
        jnp.transpose(xdt_ref[:, g * span : (g + 1) * span].astype(jnp.float32)).astype(jnp.bfloat16)
        for g in range(groups)]

    def new_copy(s):
        return pltpu.make_async_copy(
            new.at[s], states_out.at[s, pl.ds(1, props)], new_sem.at[s])

    for s in range(seqs):
        for g in range(groups):
            b = b_ref[:, g * state : (g + 1) * state].astype(jnp.float32)
            masked = jnp.concatenate(
                [jnp.where(row == t * seqs + s, b, 0.0) for t in range(props)],
                axis=1).astype(jnp.bfloat16)
            outer = dot(turned[g], masked)
            for h in range(per):
                head = g * per + h
                now = s0_ref[s, head]
                for t in range(props):
                    now = a_smem[t * seqs + s, head] * now + outer[
                        h * size : (h + 1) * size, t * state : (t + 1) * state]
                    new[s, t, head] = now
        new_copy(s).start()
    for copy in copies:
        copy.wait()
    for s in range(seqs):
        new_copy(s).wait()


def local(
    hidden, input_gain, x_weight, z_weight, bc_weight, dt_weight, x_kernel, bc_kernel,
    dt_bias, decay_log, skip_scale, output_gain, output_weight, saved_states,
    x_history, bc_history, accepted,
):
    heads = dt_bias.shape[0]
    seqs, kept, _, size, state = saved_states.shape
    hist = x_history.shape[1]
    tokens, depth = hidden.shape
    inner, bcw = x_weight.shape[1], bc_weight.shape[1]
    n_kv, n_tp = lax.axis_size("kv"), lax.axis_size("tp")
    rows = tokens // n_tp
    props = rows // seqs
    block = output_weight.shape[1] // n_kv
    n_big = 3 * inner // CHUNK
    f32, bf16 = jnp.float32, jnp.bfloat16

    vmem = pl.BlockSpec(memory_space=pltpu.VMEM)
    anym = pl.BlockSpec(memory_space=pl.ANY)
    smem = pl.BlockSpec(memory_space=pltpu.SMEM)
    dma = pltpu.SemaphoreType.DMA
    shapes = (
        ((rows, block), bf16), ((seqs, heads, size, state), f32), ((rows, inner), bf16),
        ((rows, bcw // 2), bf16), ((rows, 128), f32), ((hist, seqs, inner), bf16),
        ((hist, seqs, bcw), bf16))
    middle = pl.pallas_call(
        functools.partial(main_kernel, depth * n_tp, inner * n_kv, n_kv),
        out_shape=tuple(pltpu.VMEM(*s) for s in shapes),
        in_specs=[smem] * 4 + [anym, vmem] + [anym] * 4 + [vmem] * 5 + [anym] * 2,
        out_specs=[vmem] * len(shapes),
        scratch_shapes=[
            pltpu.VMEM((tokens, depth), bf16),
            pltpu.VMEM((depth // 128, tokens, 128), f32),
            pltpu.VMEM((128, depth), bf16),
            pltpu.VMEM((n_big, depth, CHUNK), bf16),
            pltpu.VMEM((n_tp, rows, 128), bf16),
            pltpu.VMEM((n_big, n_tp, rows, CHUNK), bf16),
            pltpu.VMEM((2, rows, 128), bf16),
            pltpu.VMEM((n_big, 2, rows, CHUNK), bf16),
            pltpu.VMEM((rows, 128), bf16),
            pltpu.VMEM((n_big, rows, CHUNK), bf16),
            pltpu.VMEM((rows, 128), f32),
            pltpu.VMEM((n_big, rows, CHUNK), f32),
            pltpu.VMEM((rows, 128), bf16),
            pltpu.VMEM((n_big, rows, CHUNK), bf16),
            pltpu.VMEM((n_kv, inner, block), bf16),
            pltpu.VMEM((n_kv - 1, rows, block), bf16),
            pltpu.VMEM((n_kv - 1, rows, block), bf16),
            pltpu.VMEM((1, 128), f32),
            pltpu.VMEM((n_kv - 1, 1, 128), f32),
            pltpu.VMEM((block // 128, rows, 128), f32),
            dma((2,)), dma((n_big,)), dma((seqs,)), dma((n_kv,)),
            dma((n_big + 1,)), dma((n_big + 1,)), dma((n_big + 1,)), dma((n_big + 1,)),
            dma((n_kv - 1,)), dma((n_kv - 1,)), dma((n_kv - 1,)), dma((n_kv - 1,)),
        ] + [pltpu.VMEM((kept, heads, size, state), f32)] * seqs,
        compiler_params=pltpu.CompilerParams(
            vmem_limit_bytes=48 << 20, collective_id=0, has_side_effects=True),
        cost_estimate=pl.CostEstimate(
            flops=2 * tokens * depth * 3 * inner, bytes_accessed=36 << 20, transcendentals=0),
        name="mixer",
    )(
        accepted, dt_bias, decay_log, skip_scale,
        hidden, input_gain, x_weight, z_weight, bc_weight, dt_weight.T,
        x_history.transpose(1, 0, 2), bc_history.transpose(1, 0, 2),
        x_kernel, bc_kernel, output_gain, saved_states, output_weight,
    )
    mixed, new_states, xw, bcw_out = pl.pallas_call(
        write_kernel,
        out_shape=(
            jax.ShapeDtypeStruct((rows, block), bf16),
            jax.ShapeDtypeStruct(saved_states.shape, f32),
            jax.ShapeDtypeStruct((hist, seqs, inner), bf16),
            jax.ShapeDtypeStruct((hist, seqs, bcw), bf16)),
        in_specs=[vmem] * len(shapes),
        out_specs=[anym] * 4,
        scratch_shapes=[
            pltpu.SMEM((rows, 128), f32),
            pltpu.VMEM((seqs, props, heads, size, state), f32),
            dma, dma((3,)), dma((seqs,)), dma((seqs,)),
        ],
        compiler_params=pltpu.CompilerParams(vmem_limit_bytes=32 << 20),
        cost_estimate=pl.CostEstimate(
            flops=2 * saved_states.size, bytes_accessed=6 * saved_states.size, transcendentals=0),
        name="write",
    )(*[pltpu.with_memory_space_constraint(v, pltpu.VMEM) for v in middle])
    return (mixed, new_states, xw.transpose(1, 0, 2), bcw_out.transpose(1, 0, 2))


def fits(mesh):
    n_kv, n_tp = mesh.shape["kv"], mesh.shape["tp"]
    inner = INNER // n_kv
    return inner % 1024 == 0 and n_kv > 1 and n_kv & (n_kv - 1) == 0 and n_tp == 4


def solution(mesh):
    in_specs = (
        P(None, "tp"),
        P("tp"),
        P("tp", "kv"),
        P("tp", "kv"),
        P("tp", "kv"),
        P("tp", "kv"),
        P(None, "kv"),
        P(None, "kv"),
        P("kv"),
        P("kv"),
        P("kv"),
        P("kv"),
        P("kv", None),
        P("tp", None, "kv", None, None),
        P("tp", None, "kv"),
        P("tp", None, "kv"),
        P("tp"),
    )
    out_specs = (
        P("tp", "kv"),
        P("tp", None, "kv", None, None),
        P("tp", None, "kv"),
        P("tp", None, "kv"),
    )
    body = local if fits(mesh) else local_general
    return jax.shard_map(body, mesh=mesh, in_specs=in_specs, out_specs=out_specs, check_vma=False)
```

time: 59.8 us -> 44.4 us (0.74)
  Pallas kernels: 47.7 us -> 34.4 us
  local copies, waits for them, and re-layouts: 3.01 us -> 8.87 us
  matrix products: 5.59 us -> 0 us
  other arithmetic: 1.83 us -> 0 us
    pallas_call x4 -> x2, Pallas kernels: 47.7 us -> 34.4 us  [the longest x1 27.1 us: local(): pl.pallas_call(functools.partial(main_kernel, depth * n_tp, inner * n_kv,...]
    unnamed x4 -> x24, local copies, waits for them, and re-layouts: 1.54 us -> 8.87 us
    dot_general x1 -> x0, matrix products: 5.59 us -> none  [local(): jnp.dot(entry, weights, preferred_element_type=jnp.float32)]
    concatenate x1 -> x0, local copies, waits for them, and re-layouts: 1.46 us -> none  [local(): jnp.concatenate([product, fill], axis=1).reshape(n_tp, rows, -1)]
    reduce_sum x1 -> x0, other arithmetic: 1.09 us -> none  [local(): squares = jnp.sum(widened * widened, axis=1, keepdims=True)]
    convert_element_type x1 -> x0, other arithmetic: 0.69 us -> none  [local(): entry = (widened * input_gain.astype(jnp.float32)).astype(jnp.bfloat16)]
where the time goes in v1:
time: 44.4 us; the launch traced here: 44 us
  Pallas kernels  34.4 us (77%)
  local copies, waits for them, and re-layouts  8.87 us (20%)
  between operations  0.67 us (2%)
    pallas_call x1, Pallas kernels, local(): pl.pallas_call(functools.partial(main_kernel, depth * n_tp, inner * n_kv,...  27.1 us
    unnamed x24, local copies, waits for them, and re-layouts  8.87 us
    pallas_call x1, Pallas kernels, local(): pl.pallas_call(write_kernel, out_shape=(jax.ShapeDtypeStruct((rows, block...  7.38 us

profile of v1, /device:TPU:0, one launch (start us, length us, event | category | flops | bytes accessed | tf_op | source)
XLA Modules:
  0.0 44.0 jit_solution(430863685259547996)
XLA Ops:
  0.6 0.0 copy-start
  0.6 0.9 %copy-done = bf16[128,1024]{1,0:T(8,128)(2,1)S(1)} copy-done((bf16[128,1024]{1,0:T(8,128)(2,1)S(1)}, bf16[128,1024]{1,0:T(8,128)(2,1)}, u32[]{:S(2)}) %copy-start) | copy-done | bytes 262168
  1.6 0.0 copy-start.1
  1.6 0.9 %copy-done.1 = bf16[8,7,1024]{2,0,1:T(8,128)(2,1)S(1)} copy-done((bf16[8,7,1024]{2,0,1:T(8,128)(2,1)S(1)}, bf16[8,7,1024]{2,0,1:T(8,128)(2,1)}, u32[]{:S(2)}) %copy-start.1) | copy-done | bytes 114712
  2.5 0.0 copy-start.2
  2.5 0.9 %copy-done.2 = bf16[8,7,1024]{2,0,1:T(8,128)(2,1)S(1)} copy-done((bf16[8,7,1024]{2,0,1:T(8,128)(2,1)S(1)}, bf16[8,7,1024]{2,0,1:T(8,128)(2,1)}, u32[]{:S(2)}) %copy-start.2) | copy-done | bytes 114712
  3.4 0.0 copy-start.3
  3.4 0.8 %copy-done.3 = bf16[1024,16]{0,1:T(8,128)(2,1)S(1)} copy-done((bf16[1024,16]{0,1:T(8,128)(2,1)S(1)}, bf16[1024,16]{0,1:T(8,128)(2,1)}, u32[]{:S(2)}) %copy-start.3) | copy-done | bytes 32792
  4.1 0.0 copy-start.4
  4.1 0.7 %copy-done.4 = bf16[4,1024]{1,0:T(4,128)(2,1)S(1)} copy-done((bf16[4,1024]{1,0:T(4,128)(2,1)S(1)}, bf16[4,1024]{1,0:T(4,128)(2,1)}, u32[]{:S(2)}) %copy-start.4) | copy-done | bytes 8216
  4.8 0.0 copy-start.5
  4.8 0.7 %copy-done.5 = bf16[4,1024]{1,0:T(4,128)(2,1)S(1)} copy-done((bf16[4,1024]{1,0:T(4,128)(2,1)S(1)}, bf16[4,1024]{1,0:T(4,128)(2,1)}, u32[]{:S(2)}) %copy-start.5) | copy-done | bytes 8216
  5.5 0.0 copy-start.6
  5.5 0.7 %copy-done.6 = bf16[1024]{0:T(1024)(128)(2,1)S(1)} copy-done((bf16[1024]{0:T(1024)(128)(2,1)S(1)}, bf16[1024]{0:T(1024)(128)(2,1)}, u32[]{:S(2)}) %copy-start.6) | copy-done | bytes 2072
  6.2 0.0 copy-start.7
  6.2 0.7 %copy-done.7 = bf16[1024]{0:T(1024)(128)(2,1)S(1)} copy-done((bf16[1024]{0:T(1024)(128)(2,1)S(1)}, bf16[1024]{0:T(1024)(128)(2,1)}, u32[]{:S(2)}) %copy-start.7) | copy-done | bytes 2072
  6.9 0.0 copy-start.8
  6.9 0.7 %copy-done.8 = s32[8]{0:T(128)S(1)} copy-done((s32[8]{0:T(128)S(1)}, s32[8]{0:T(128)}, u32[]{:S(2)}) %copy-start.8) | copy-done | bytes 56
  7.6 0.0 copy-start.9
  7.6 0.7 %copy-done.9 = f32[16]{0:T(128)S(1)} copy-done((f32[16]{0:T(128)S(1)}, f32[16]{0:T(128)}, u32[]{:S(2)}) %copy-start.9) | copy-done | bytes 88
  8.2 0.0 copy-start.10
  8.2 0.7 %copy-done.10 = f32[16]{0:T(128)S(1)} copy-done((f32[16]{0:T(128)S(1)}, f32[16]{0:T(128)}, u32[]{:S(2)}) %copy-start.10) | copy-done | bytes 88
  8.9 0.0 copy-start.11
  8.9 0.7 %copy-done.11 = f32[16]{0:T(128)S(1)} copy-done((f32[16]{0:T(128)S(1)}, f32[16]{0:T(128)}, u32[]{:S(2)}) %copy-start.11) | copy-done | bytes 88
  9.5 27.1 %mixer.1 = (bf16[32,512]{1,0:T(8,128)(2,1)S(1)}, f32[8,16,64,128]{3,2,1,0:T(8,128)S(1)}, bf16[32,1024]{1,0:T(8,128)(2,1)S(1)}, bf16[32,512]{1,0:T(8,128)(2,1)S(1...) custom-call(s32[8]{0:T(128)S(1)} %copy-done.8, f32[16]{0:T(128)S(1)} %copy-done.9, ...), custom_call_target="tpu_custom_call" | custom-call | flops 805306368 | bytes 37748736 | tf_op jit(solution)/shard_map/mixer/pallas_call | solution.py:531
  36.6 7.4 %write.1 = (bf16[32,512]{1,0:T(8,128)(2,1)}, f32[8,5,16,64,128]{4,3,2,1,0:T(8,128)}, bf16[7,8,1024]{2,1,0:T(8,128)(2,1)}, bf16[7,8,1024]{2,1,0:T(8,128)(2,1)}) custom-call(bf16[32,512]{1,0:T(8,128)(2,1)S(1)} %get-tuple-element.15.mixed_ref, f32[8,16,64,128]{3,2,1,0:T(8,128)S(1)} %get-tuple-element.16.s0_ref, bf16[32,1024]{1,0:T(8,128)(2,1)S(1)} %get-tuple-element.17.xdt_ref, ...), custom_call_target="tpu_custom_call" | custom-call | flops 10485760 | bytes 31457280 | tf_op jit(solution)/shard_map/write/pallas_call | solution.py:572
Async XLA Ops:
  0.6 1.0 %copy-start = (bf16[128,1024]{1,0:T(8,128)(2,1)S(1)}, bf16[128,1024]{1,0:T(8,128)(2,1)}, u32[]{:S(2)}) copy-start(bf16[128,1024]{1,0:T(8,128)(2,1)} %hid_hbm.1) | copy-start | bytes 786436
  1.6 0.9 %copy-start.1 = (bf16[8,7,1024]{2,0,1:T(8,128)(2,1)S(1)}, bf16[8,7,1024]{2,0,1:T(8,128)(2,1)}, u32[]{:S(2)}) copy-start(bf16[8,7,1024]{2,0,1:T(8,128)(2,1)} %param.31) | copy-start | bytes 344068
  2.5 0.9 %copy-start.2 = (bf16[8,7,1024]{2,0,1:T(8,128)(2,1)S(1)}, bf16[8,7,1024]{2,0,1:T(8,128)(2,1)}, u32[]{:S(2)}) copy-start(bf16[8,7,1024]{2,0,1:T(8,128)(2,1)} %param.32) | copy-start | bytes 344068
  3.4 0.8 %copy-start.3 = (bf16[1024,16]{0,1:T(8,128)(2,1)S(1)}, bf16[1024,16]{0,1:T(8,128)(2,1)}, u32[]{:S(2)}) copy-start(bf16[1024,16]{0,1:T(8,128)(2,1)} %param.22) | copy-start | bytes 98308
  4.1 0.7 %copy-start.4 = (bf16[4,1024]{1,0:T(4,128)(2,1)S(1)}, bf16[4,1024]{1,0:T(4,128)(2,1)}, u32[]{:S(2)}) copy-start(bf16[4,1024]{1,0:T(4,128)(2,1)} %xk_ref.1) | copy-start | bytes 24580
  4.8 0.7 %copy-start.5 = (bf16[4,1024]{1,0:T(4,128)(2,1)S(1)}, bf16[4,1024]{1,0:T(4,128)(2,1)}, u32[]{:S(2)}) copy-start(bf16[4,1024]{1,0:T(4,128)(2,1)} %bck_ref.1) | copy-start | bytes 24580
  5.5 0.7 %copy-start.6 = (bf16[1024]{0:T(1024)(128)(2,1)S(1)}, bf16[1024]{0:T(1024)(128)(2,1)}, u32[]{:S(2)}) copy-start(bf16[1024]{0:T(1024)(128)(2,1)} %gin_ref.1) | copy-start | bytes 6148
  6.2 0.7 %copy-start.7 = (bf16[1024]{0:T(1024)(128)(2,1)S(1)}, bf16[1024]{0:T(1024)(128)(2,1)}, u32[]{:S(2)}) copy-start(bf16[1024]{0:T(1024)(128)(2,1)} %gain_ref.1) | copy-start | bytes 6148
  6.9 0.7 %copy-start.8 = (s32[8]{0:T(128)S(1)}, s32[8]{0:T(128)}, u32[]{:S(2)}) copy-start(s32[8]{0:T(128)} %acc_smem.1) | copy-start | bytes 100
  7.6 0.7 %copy-start.9 = (f32[16]{0:T(128)S(1)}, f32[16]{0:T(128)}, u32[]{:S(2)}) copy-start(f32[16]{0:T(128)} %bias_smem.1) | copy-start | bytes 196
  8.2 0.7 %copy-start.10 = (f32[16]{0:T(128)S(1)}, f32[16]{0:T(128)}, u32[]{:S(2)}) copy-start(f32[16]{0:T(128)} %decay_smem.1) | copy-start | bytes 196
  8.9 0.7 %copy-start.11 = (f32[16]{0:T(128)S(1)}, f32[16]{0:T(128)}, u32[]{:S(2)}) copy-start(f32[16]{0:T(128)} %skip_smem.1) | copy-start | bytes 196

commit v2 on v1

--- a/solution.py
+++ b/solution.py
@@ -146,7 +146,8 @@
 NN = (((1,), (0,)), ((), ()))
 NT = (((1,), (1,)), ((), ()))
 CHUNK = 512
-LAG = 3
+LAG = 2
+AHEAD = 4
 
 
 def dot(a, b, dims=NN, **kw):
@@ -179,13 +180,14 @@
 
 def main_kernel(
     features, channels, n_kv,
-    acc_smem, bias_smem, decay_smem, skip_smem,
-    hid_hbm, gin_ref, xw_hbm, zw_hbm, bcw_hbm, dtw_hbm, xh_ref, bch_ref, xk_ref, bck_ref, gain_ref,
+    acc_hbm, bias_hbm, decay_hbm, skip_hbm,
+    hid_hbm, gin_hbm, xw_hbm, zw_hbm, bcw_hbm, dtw_hbm, xh_hbm, bch_hbm, xk_hbm, bck_hbm, gain_hbm,
     saved_hbm, w_hbm,
     mixed_ref, s0_ref, xdt_ref, b_ref, a_ref, xwin_ref, bcwin_ref,
+    acc_smem, bias_smem, decay_smem, skip_smem, gin_ref, xh_ref, bch_ref, xk_ref, bck_ref, gain_ref,
     hid, entry32, dtw, wbuf, prod_dt, prod, peer_dt, peer, half_dt, half, own_dt, own, far_dt, far,
     w_buf, part, slots, norm_out, norm_in, fin,
-    hid_sem, w_sem, saved_sem, ow_sem, c_send, c_recv, x_send, x_recv, o_send, o_recv, n_send, n_recv,
+    hid_sem, small_sem, w_sem, saved_sem, ow_sem, c_send, c_recv, x_send, x_recv, o_send, o_recv, n_send, n_recv,
     *saved,
 ):
     seqs = acc_smem.shape[0]
@@ -204,7 +206,9 @@
     kv, tp = lax.axis_index("kv"), lax.axis_index("tp")
     side, core = tp // 2, lax.rem(tp, 2)
     core_peer, x_peer = flip(tp, 1), flip(tp, 2)
-    exits = [flip(kv, d) for d in range(n_kv - 1, 0, -1)]
+    ranks = list(range(0, n_kv - 1, 2))
+    ranks = ranks[: len(ranks) // 2] + ranks[: len(ranks) // 2 - 1 : -1] + list(range(1, n_kv - 1, 2))
+    exits = [i + (i - kv + n_kv) // n_kv for i in ranks]
 
     barrier = pltpu.get_barrier_semaphore()
     for device in [{"tp": core_peer}, {"tp": x_peer}] + [{"kv": p} for p in exits]:
@@ -212,7 +216,9 @@
 
     hid_copy = pltpu.make_async_copy(hid_hbm, hid, hid_sem.at[0])
     hid_copy.start()
-    dtw_copy = pltpu.make_async_copy(dtw_hbm, dtw.at[pl.ds(0, heads)], hid_sem.at[1])
+    gin_copy = pltpu.make_async_copy(gin_hbm, gin_ref, hid_sem.at[1])
+    gin_copy.start()
+    dtw_copy = pltpu.make_async_copy(dtw_hbm, dtw.at[pl.ds(0, heads)], hid_sem.at[2])
     dtw_copy.start()
     w_copies = [
         pltpu.make_async_copy(src.at[:, pl.ds(j * CHUNK, CHUNK)], wbuf.at[i], w_sem.at[i])
@@ -221,6 +227,14 @@
     ]
     for copy in w_copies:
         copy.start()
+    small_copies = [
+        pltpu.make_async_copy(src, dst, small_sem.at[i])
+        for i, (src, dst) in enumerate([
+            (acc_hbm, acc_smem), (bias_hbm, bias_smem), (decay_hbm, decay_smem), (skip_hbm, skip_smem),
+            (xh_hbm, xh_ref), (bch_hbm, bch_ref), (xk_hbm, xk_ref), (bck_hbm, bck_ref),
+            (gain_hbm, gain_ref)])]
+    for copy in small_copies:
+        copy.start()
     n_big = len(w_copies)
 
     dtw[heads:] = jnp.zeros((dtw.shape[0] - heads, dtw.shape[1]), dtw.dtype)
@@ -228,6 +242,7 @@
     lanes = entry32.shape[2]
     for i in range(entry32.shape[0]):
         entry32[i] = hid[:, i * lanes : (i + 1) * lanes].astype(jnp.float32)
+    gin_copy.wait()
     gin = gin_ref[...].astype(jnp.float32).reshape(1, -1)
     entry, squares = [], []
     for p in range(tokens // rows):
@@ -283,12 +298,14 @@
         core_copy(k).start()
         if k >= LAG - 1:
             forward(k - LAG)
-        if k == n_big - 1:
-            for copy in saved_copies + ow_copies:
+        if k == 0:
+            for copy in saved_copies:
                 copy.start()
     for k in range(n_big - LAG, n_big):
         forward(k)
 
+    for copy in small_copies:
+        copy.wait()
     seq_at = lax.broadcasted_iota(jnp.int32, (seqs, CHUNK), 0)
     acc = jnp.zeros((seqs, CHUNK), jnp.int32)
     for s in range(seqs):
@@ -360,16 +377,6 @@
             pairs.append({
                 (t, r): jnp.broadcast_to(jnp.sum(c[t] * b[r], axis=1, keepdims=True), (seqs, span))
                 for t in range(props) for r in range(t + 1)})
-
-    carried = [jnp.zeros((rows, span), jnp.float32) for _ in range(groups)]
-    for s in range(seqs):
-        saved_copies[s].wait()
-        s0 = saved[s][acc_smem[s]]
-        s0_ref[s] = s0
-        low = s0.reshape(heads * size, state).astype(jnp.bfloat16)
-        for g in range(groups):
-            masked = jnp.where(row % seqs == s, c_low[g].astype(jnp.float32), 0.0).astype(jnp.bfloat16)
-            carried[g] = carried[g] + dot(masked, low[g * span : (g + 1) * span], NT)
 
     outs, gated_parts = [], []
     for j in range(n_chunk):
@@ -393,10 +400,22 @@
                 else:
                     out = out + jnp.exp(gap) * pair * xdt[r]
                     gap = gap + decays[r]
-            held = jnp.concatenate(
-                [carried[j * in_chunk + i][t * seqs : (t + 1) * seqs] for i in range(in_chunk)], axis=1)
-            out_t.append(out + jnp.exp(gap) * held)
+            out_t.append((out, jnp.exp(gap)))
         outs.append(out_t)
+
+    carried = [jnp.zeros((rows, span), jnp.float32) for _ in range(groups)]
+    for s in range(seqs):
+        saved_copies[s].wait()
+        if s == seqs - AHEAD:
+            for copy in ow_copies:
+                copy.start()
+        s0 = saved[s][acc_smem[s]]
+        s0_ref[s] = s0
+        low = s0.reshape(heads * size, state).astype(jnp.bfloat16)
+        for g in range(groups):
+            masked = jnp.where(row % seqs == s, c_low[g].astype(jnp.float32), 0.0).astype(jnp.bfloat16)
+            carried[g] = carried[g] + dot(masked, low[g * span : (g + 1) * span], NT)
+
     square_sums = [jnp.zeros((seqs, 1), jnp.float32) for _ in range(props)]
     gain = gain_ref[...].astype(jnp.float32).reshape(1, inner)
     for j in range(n_chunk):
@@ -404,7 +423,10 @@
         zs = fresh(2 * n_chunk + j)
         scaled_t = []
         for t in range(props):
-            v = outs[j][t] * silu(zs[t])
+            held = jnp.concatenate(
+                [carried[j * in_chunk + i][t * seqs : (t + 1) * seqs] for i in range(in_chunk)], axis=1)
+            out, fade = outs[j][t]
+            v = (out + fade * held) * silu(zs[t])
             square_sums[t] = square_sums[t] + jnp.sum(v * v, axis=1, keepdims=True)
             scaled_t.append((v * gain[:, sl]).astype(jnp.bfloat16))
         gated_parts.append(jnp.concatenate(scaled_t, axis=0))
@@ -416,28 +438,35 @@
         jnp.where(diagonal, jnp.concatenate(square_sums, axis=0), 0.0), axis=0, keepdims=True)
     norm_out[...] = norm_row
     n_copies = [
-        remote(norm_out, norm_in.at[i], n_send.at[i], n_recv.at[i], {"kv": p})
+        remote(norm_out, norm_in.at[kv], n_send.at[i], n_recv.at[kv], {"kv": p})
         for i, p in enumerate(exits)]
     for copy in n_copies:
         copy.start()
     o_copies = [
-        remote(part.at[i], slots.at[i], o_send.at[i], o_recv.at[i], {"kv": p})
+        remote(part.at[i], slots.at[kv], o_send.at[i], o_recv.at[kv], {"kv": p})
         for i, p in enumerate(exits)]
+    sources = [flip(kv, d) for d in range(1, n_kv)]
+
+    def arrived(p):
+        remote(norm_out, norm_in.at[p], n_send.at[0], n_recv.at[p], {"kv": p}).wait_recv()
+
+    def landed(p):
+        remote(part.at[0], slots.at[p], o_send.at[0], o_recv.at[p], {"kv": p}).wait_recv()
+
     for i in range(n_kv):
         ow_copies[i].wait()
         value = dot(scaled, w_buf[i])
         if i < n_kv - 1:
             part[i] = value.astype(jnp.bfloat16)
             o_copies[i].start()
-    for copy in n_copies:
-        copy.wait_recv()
-    for i in range(n_kv - 1):
-        norm_row = norm_row + norm_in[i]
+    for p in sources:
+        arrived(p)
+        norm_row = norm_row + norm_in[p]
     norm = lax.rsqrt(
         jnp.sum(jnp.where(diagonal, norm_row, 0.0), axis=1, keepdims=True) / channels + EPSILON)
-    for i in range(n_kv - 2, -1, -1):
-        o_copies[i].wait_recv()
-        value = value + slots[i].astype(jnp.float32)
+    for p in sources:
+        landed(p)
+        value = value + slots[p].astype(jnp.float32)
     value = value * norm
     for i in range(fin.shape[0]):
         for t in range(props):
@@ -522,7 +551,6 @@
 
     vmem = pl.BlockSpec(memory_space=pltpu.VMEM)
     anym = pl.BlockSpec(memory_space=pl.ANY)
-    smem = pl.BlockSpec(memory_space=pltpu.SMEM)
     dma = pltpu.SemaphoreType.DMA
     shapes = (
         ((rows, block), bf16), ((seqs, heads, size, state), f32), ((rows, inner), bf16),
@@ -531,9 +559,19 @@
     middle = pl.pallas_call(
         functools.partial(main_kernel, depth * n_tp, inner * n_kv, n_kv),
         out_shape=tuple(pltpu.VMEM(*s) for s in shapes),
-        in_specs=[smem] * 4 + [anym, vmem] + [anym] * 4 + [vmem] * 5 + [anym] * 2,
+        in_specs=[pl.BlockSpec(memory_space=pltpu.HBM)] * 17,
         out_specs=[vmem] * len(shapes),
         scratch_shapes=[
+            pltpu.SMEM((seqs,), jnp.int32),
+            pltpu.SMEM((heads,), f32),
+            pltpu.SMEM((heads,), f32),
+            pltpu.SMEM((heads,), f32),
+            pltpu.VMEM((depth,), bf16),
+            pltpu.VMEM((hist, seqs, inner), bf16),
+            pltpu.VMEM((hist, seqs, bcw), bf16),
+            pltpu.VMEM(x_kernel.shape, bf16),
+            pltpu.VMEM(bc_kernel.shape, bf16),
+            pltpu.VMEM((inner,), bf16),
             pltpu.VMEM((tokens, depth), bf16),
             pltpu.VMEM((depth // 128, tokens, 128), f32),
             pltpu.VMEM((128, depth), bf16),
@@ -550,25 +588,25 @@
             pltpu.VMEM((n_big, rows, CHUNK), bf16),
             pltpu.VMEM((n_kv, inner, block), bf16),
             pltpu.VMEM((n_kv - 1, rows, block), bf16),
-            pltpu.VMEM((n_kv - 1, rows, block), bf16),
+            pltpu.VMEM((n_kv, rows, block), bf16),
             pltpu.VMEM((1, 128), f32),
-            pltpu.VMEM((n_kv - 1, 1, 128), f32),
+            pltpu.VMEM((n_kv, 1, 128), f32),
             pltpu.VMEM((block // 128, rows, 128), f32),
-            dma((2,)), dma((n_big,)), dma((seqs,)), dma((n_kv,)),
+            dma((3,)), dma((9,)), dma((n_big,)), dma((seqs,)), dma((n_kv,)),
             dma((n_big + 1,)), dma((n_big + 1,)), dma((n_big + 1,)), dma((n_big + 1,)),
-            dma((n_kv - 1,)), dma((n_kv - 1,)), dma((n_kv - 1,)), dma((n_kv - 1,)),
+            dma((n_kv - 1,)), dma((n_kv,)), dma((n_kv - 1,)), dma((n_kv,)),
         ] + [pltpu.VMEM((kept, heads, size, state), f32)] * seqs,
         compiler_params=pltpu.CompilerParams(
             vmem_limit_bytes=48 << 20, collective_id=0, has_side_effects=True),
         cost_estimate=pl.CostEstimate(
             flops=2 * tokens * depth * 3 * inner, bytes_accessed=36 << 20, transcendentals=0),
         name="mixer",
-    )(
+    )(*[pltpu.with_memory_space_constraint(v, pltpu.HBM) for v in (
         accepted, dt_bias, decay_log, skip_scale,
         hidden, input_gain, x_weight, z_weight, bc_weight, dt_weight.T,
         x_history.transpose(1, 0, 2), bc_history.transpose(1, 0, 2),
         x_kernel, bc_kernel, output_gain, saved_states, output_weight,
-    )
+    )])
     mixed, new_states, xw, bcw_out = pl.pallas_call(
         write_kernel,
         out_shape=(

time: 44.4 us -> 29.4 us (0.66)
  local copies, waits for them, and re-layouts: 8.87 us -> 0 us
  Pallas kernels: 34.4 us -> 28.2 us
    unnamed x24 -> x0, local copies, waits for them, and re-layouts: 8.87 us -> none
    pallas_call x1, Pallas kernels: 27.1 us -> 20.8 us  [local(): pl.pallas_call(functools.partial(main_kernel, depth * n_tp, inner * n_kv,...]
where the time goes in v2:
time: 29.4 us; the launch traced here: 28.9 us
  Pallas kernels  28.2 us (96%)
  between operations  0.65 us (2%)
    pallas_call x1, Pallas kernels, local(): pl.pallas_call(functools.partial(main_kernel, depth * n_tp, inner * n_kv,...  20.8 us
    pallas_call x1, Pallas kernels, local(): pl.pallas_call(write_kernel, out_shape=(jax.ShapeDtypeStruct((rows, block...  7.38 us

profile of v2, /device:TPU:0, one launch (start us, length us, event | category | flops | bytes accessed | tf_op | source)
XLA Modules:
  0.0 28.9 jit_solution(11496499023687157229)
XLA Ops:
  0.6 20.8 %mixer.1 = (bf16[32,512]{1,0:T(8,128)(2,1)S(1)}, f32[8,16,64,128]{3,2,1,0:T(8,128)S(1)}, bf16[32,1024]{1,0:T(8,128)(2,1)S(1)}, bf16[32,512]{1,0:T(8,128)(2,1)S(1...) custom-call(s32[8]{0:T(128)} %acc_hbm.1, f32[16]{0:T(128)} %bias_hbm.1, ...), custom_call_target="tpu_custom_call" | custom-call | flops 805306368 | bytes 37748736 | tf_op jit(solution)/shard_map/mixer/pallas_call | solution.py:559
  21.5 7.4 %write.1 = (bf16[32,512]{1,0:T(8,128)(2,1)}, f32[8,5,16,64,128]{4,3,2,1,0:T(8,128)}, bf16[7,8,1024]{2,1,0:T(8,128)(2,1)}, bf16[7,8,1024]{2,1,0:T(8,128)(2,1)}) custom-call(bf16[32,512]{1,0:T(8,128)(2,1)S(1)} %get-tuple-element.15.mixed_ref, f32[8,16,64,128]{3,2,1,0:T(8,128)S(1)} %get-tuple-element.16.s0_ref, bf16[32,1024]{1,0:T(8,128)(2,1)S(1)} %get-tuple-element.17.xdt_ref, ...), custom_call_target="tpu_custom_call" | custom-call | flops 10485760 | bytes 31457280 | tf_op jit(solution)/shard_map/write/pallas_call | solution.py:610

commit v3 on v2

--- a/solution.py
+++ b/solution.py
@@ -10,7 +10,6 @@
 D = 4096
 PROPS = 4
 INNER = 8192
-
 
 EPSILON = 1e-05
 
@@ -142,12 +141,10 @@
     mixed = (lax.rsqrt(total_squares / INNER + EPSILON)[:, None] * summed).astype(jnp.bfloat16)
     return (mixed, new_states, x_window, bc_window)
 
-
 NN = (((1,), (0,)), ((), ()))
 NT = (((1,), (1,)), ((), ()))
 CHUNK = 512
 LAG = 2
-AHEAD = 4
 
 
 def dot(a, b, dims=NN, **kw):
@@ -210,16 +207,16 @@
     ranks = ranks[: len(ranks) // 2] + ranks[: len(ranks) // 2 - 1 : -1] + list(range(1, n_kv - 1, 2))
     exits = [i + (i - kv + n_kv) // n_kv for i in ranks]
 
-    barrier = pltpu.get_barrier_semaphore()
-    for device in [{"tp": core_peer}, {"tp": x_peer}] + [{"kv": p} for p in exits]:
-        pl.semaphore_signal(barrier, inc=1, device_id=device, device_id_type=pl.DeviceIdType.MESH)
-
     hid_copy = pltpu.make_async_copy(hid_hbm, hid, hid_sem.at[0])
     hid_copy.start()
     gin_copy = pltpu.make_async_copy(gin_hbm, gin_ref, hid_sem.at[1])
     gin_copy.start()
     dtw_copy = pltpu.make_async_copy(dtw_hbm, dtw.at[pl.ds(0, heads)], hid_sem.at[2])
     dtw_copy.start()
+    barrier = pltpu.get_barrier_semaphore()
+    for device in [{"tp": core_peer}, {"tp": x_peer}] + [{"kv": p} for p in exits]:
+        pl.semaphore_signal(barrier, inc=1, device_id=device, device_id_type=pl.DeviceIdType.MESH)
+
     w_copies = [
         pltpu.make_async_copy(src.at[:, pl.ds(j * CHUNK, CHUNK)], wbuf.at[i], w_sem.at[i])
         for i, (src, j) in enumerate(
@@ -303,6 +300,8 @@
                 copy.start()
     for k in range(n_big - LAG, n_big):
         forward(k)
+    for copy in ow_copies:
+        copy.start()
 
     for copy in small_copies:
         copy.wait()
@@ -406,9 +405,6 @@
     carried = [jnp.zeros((rows, span), jnp.float32) for _ in range(groups)]
     for s in range(seqs):
         saved_copies[s].wait()
-        if s == seqs - AHEAD:
-            for copy in ow_copies:
-                copy.start()
         s0 = saved[s][acc_smem[s]]
         s0_ref[s] = s0
         low = s0.reshape(heads * size, state).astype(jnp.bfloat16)

time: 29.4 us -> 28.9 us (0.983)
  Pallas kernels: 28.2 us -> 27.9 us
    pallas_call x1, Pallas kernels: 20.8 us -> 20.5 us  [local(): pl.pallas_call(functools.partial(main_kernel, depth * n_tp, inner * n_kv,...]
where the time goes in v3:
time: 28.9 us; the launch traced here: 28.5 us
  Pallas kernels  27.9 us (97%)
  between operations  0.65 us (2%)
    pallas_call x1, Pallas kernels, local(): pl.pallas_call(functools.partial(main_kernel, depth * n_tp, inner * n_kv,...  20.5 us
    pallas_call x1, Pallas kernels, local(): pl.pallas_call(write_kernel, out_shape=(jax.ShapeDtypeStruct((rows, block...  7.38 us

profile of v3, /device:TPU:0, one launch (start us, length us, event | category | flops | bytes accessed | tf_op | source)
XLA Modules:
  0.0 28.5 jit_solution(10382986102346962178)
XLA Ops:
  0.6 20.5 %mixer.1 = (bf16[32,512]{1,0:T(8,128)(2,1)S(1)}, f32[8,16,64,128]{3,2,1,0:T(8,128)S(1)}, bf16[32,1024]{1,0:T(8,128)(2,1)S(1)}, bf16[32,512]{1,0:T(8,128)(2,1)S(1...) custom-call(s32[8]{0:T(128)} %acc_hbm.1, f32[16]{0:T(128)} %bias_hbm.1, ...), custom_call_target="tpu_custom_call" | custom-call | flops 805306368 | bytes 37748736 | tf_op jit(solution)/shard_map/mixer/pallas_call | solution.py:555
  21.1 7.4 %write.1 = (bf16[32,512]{1,0:T(8,128)(2,1)}, f32[8,5,16,64,128]{4,3,2,1,0:T(8,128)}, bf16[7,8,1024]{2,1,0:T(8,128)(2,1)}, bf16[7,8,1024]{2,1,0:T(8,128)(2,1)}) custom-call(bf16[32,512]{1,0:T(8,128)(2,1)S(1)} %get-tuple-element.15.mixed_ref, f32[8,16,64,128]{3,2,1,0:T(8,128)S(1)} %get-tuple-element.16.s0_ref, bf16[32,1024]{1,0:T(8,128)(2,1)S(1)} %get-tuple-element.17.xdt_ref, ...), custom_call_target="tpu_custom_call" | custom-call | flops 10485760 | bytes 31457280 | tf_op jit(solution)/shard_map/write/pallas_call | solution.py:606
